TPU v7x, 32 devices: a whole 2x2x4 slice. The times are simulated.
32 devices in a mesh: grp: 2 (over x), fs: 4 (over z), tp: 4 (over y, core).
Axes of the slice: x: 2, y: 2, z: 4, core: 2. Of those that a mesh axis runs over, the one named last changes fastest.
Arguments:
- tokens: bfloat16 [2048, 2048], P(('grp', 'fs'), 'tp'), parts along dimension 0, may hold values from -12 to 12
- gain_first: float32 [2048], P('tp'), may hold values from 0.1 to 1.9
- gate_first: float32 [2048, 5632], P('fs', 'tp'), may hold values from -0.125 to 0.125
- gate_scale_first: float32 [5632], P('tp'), may hold values from 0.5 to 2
- up_first: float32 [2048, 5632], P('fs', 'tp'), may hold values from -0.125 to 0.125
- up_scale_first: float32 [5632], P('tp'), may hold values from 0.5 to 2
- down_first: float32 [5632, 2048], P('tp', 'fs'), may hold values from -0.078125 to 0.078125
- down_scale_first: float32 [2048], P('tp'), may hold values from 0.5 to 2
- gain_second: float32 [2048], P('tp'), may hold values from 0.1 to 1.9
- gate_second: float32 [2048, 5632], P('fs', 'tp'), may hold values from -0.125 to 0.125
- gate_scale_second: float32 [5632], P('tp'), may hold values from 0.5 to 2
- up_second: float32 [2048, 5632], P('fs', 'tp'), may hold values from -0.125 to 0.125
- up_scale_second: float32 [5632], P('tp'), may hold values from 0.5 to 2
- down_second: float32 [5632, 2048], P('tp', 'fs'), may hold values from -0.078125 to 0.078125
- down_scale_second: float32 [2048], P('tp'), may hold values from 0.5 to 2
Outputs:
- stream_out: bfloat16 [2048, 2048], P(('grp', 'fs'), 'tp'), parts along dimension 0
There are 2 independent parts, one for each index of `grp`. A program takes and returns all parts, laid end to end along the dimension named above; an argument that names none is the same for every part. Nothing has to cross between parts.
All inputs are finite; a program needn't handle non-finite values.
Results may differ from a plain program's by a relative error of at most 0.028.
Values may be sent and summed in bfloat16 or wider, within the bound.
A program may use at most 128 MiB of HBM per device.

v0:
```python
import functools

import jax
import jax.numpy as jnp
from jax import lax
from jax.experimental import pallas as pl
from jax.experimental.pallas import tpu as pltpu
from jax.sharding import PartitionSpec as P

MESH = pl.DeviceIdType.MESH
LANES = 128

epsilon = 1e-06


def normalize(stream, gain):
    values = stream.astype(jnp.float32)
    totals = lax.psum(jnp.sum(values * values, axis=1), "tp")
    width = values.shape[1] * lax.axis_size("tp")
    normed = (values * lax.rsqrt(totals / width + epsilon)[:, None] * gain).astype(jnp.bfloat16)
    return values, lax.all_gather(normed, "tp", axis=1, tiled=True)


def gathered_block(stream, gain, gate_w, gate_s, up_w, up_s, down_w, down_s):
    values, whole = normalize(stream, gain)

    def project(weight, scale):
        rows = lax.all_gather(weight.astype(jnp.bfloat16), "fs", axis=0, tiled=True)
        return jnp.dot(whole, rows, preferred_element_type=jnp.float32) * scale

    hidden = (jax.nn.silu(project(gate_w, gate_s)) * project(up_w, up_s)).astype(jnp.bfloat16)
    columns = lax.all_gather(down_w.astype(jnp.bfloat16), "fs", axis=1, tiled=True)
    terms = jnp.dot(hidden, columns, preferred_element_type=jnp.float32).astype(jnp.bfloat16)
    summed = lax.psum_scatter(terms, "tp", scatter_dimension=1, tiled=True).astype(jnp.float32)
    return (values + 0.5 * summed * down_s).astype(jnp.bfloat16)


def body_gather(tokens, *rest):
    middle = gathered_block(tokens, *rest[:7])
    return gathered_block(middle, *rest[7:])


def both_blocks(n_fs, n_tp, tiles, *refs):
    (tokens, gains, scales, down_scales), refs = refs[:4], refs[4:]
    weights, out, refs = refs[:6], refs[6], refs[7:]
    (
        wide_gate, wide_up, wide_down, all_gains,
        cols_0, cols_1, rows_0, rows_1, gu_0, gu_1, dn_0, dn_1, x_0, x_1, normed, hidden,
        core_out, from_core_0, from_core_1, y_out, from_y_0, from_y_1,
        z_out, from_left_0, from_left_1, from_right_0, from_right_1, total, kept,
        load_sem, gain_send, gain_recv,
        ag_zs, ag_zr, ag_ys, ag_yr, ag_cs, ag_cr,
        gu_zs, gu_zr, gu_xs, gu_xr, dn_zs, dn_zr, dn_xs, dn_xr,
        rs_cs, rs_cr, rs_ys, rs_yr, rs_zs, rs_lr, rs_rr,
    ) = refs
    cols, rows, gu, dn, x = (cols_0, cols_1), (rows_0, rows_1), (gu_0, gu_1), (dn_0, dn_1), (x_0, x_1)
    from_core, from_y = (from_core_0, from_core_1), (from_y_0, from_y_1)
    from_left, from_right = (from_left_0, from_left_1), (from_right_0, from_right_1)

    grp, fs, tp = lax.axis_index("grp"), lax.axis_index("fs"), lax.axis_index("tp")
    core, chip = lax.rem(tp, 2), lax.div(tp, 2)
    partner, other_core, across = {"grp": 1 - grp}, {"tp": tp + 1 - 2 * core}, {"tp": lax.rem(tp + 2, n_tp)}
    far_tp = lax.rem(tp + 2, n_tp)
    last = n_fs - 1
    base = -(-tiles // n_fs)
    short = n_fs * base - tiles
    bf, f32 = jnp.bfloat16, jnp.float32

    def first_tile(dev):
        even = jnp.minimum(dev, short)
        odd = jnp.maximum(dev - (n_fs - short), 0)
        return dev * base - (1 - core) * even - core * odd

    def has_last(dev):
        return first_tile(dev + 1) - first_tile(dev) == base

    def peer(d):
        return lax.rem(fs + d, n_fs)

    def origin(d):
        return lax.rem(fs + n_fs - d, n_fs)

    def remote(src, dst, sends, recvs, device):
        return pltpu.make_async_remote_copy(
            src_ref=src, dst_ref=dst, send_sem=sends, recv_sem=recvs, device_id=device, device_id_type=MESH
        )

    def when(cond, fn):
        if cond is None:
            fn()
        else:
            pl.when(cond)(fn)

    def gu_cond(i, dev):
        return has_last(dev) if i % base == base - 1 and short else None

    def gu_z(b, i):
        d, n = 1 + i // base, i % base
        src = cols[b].at[first_tile(peer(d)) + n, grp]
        return remote(src, gu[b].at[n, fs, grp], gu_zs.at[b, i], gu_zr.at[b, i], {"fs": peer(d)})

    def gu_x(b, i):
        d, n = 1 + i // base, i % base
        block = gu[b].at[n, origin(d), grp]
        return remote(block, block, gu_xs.at[b, i], gu_xr.at[b, i], partner)

    def gu_landed(b, i):
        d, n = 1 + i // base, i % base
        block = gu[b].at[n, origin(d), grp]
        return remote(block, block, gu_zs.at[b, i], gu_zr.at[b, i], {"fs": origin(d)})

    def dn_part(i):
        return pl.ds(0, base - 1) if i % 2 == 0 else pl.ds(base - 1, 1)

    def dn_cond(i, dev):
        return has_last(dev) if i % 2 == 1 and short else None

    def dn_z(b, i):
        d = 1 + i // 2
        start = first_tile(peer(d))
        src = pl.ds(start, base - 1) if i % 2 == 0 else pl.ds(start + base - 1, 1)
        dst = dn[b].at[fs, dn_part(i), grp]
        return remote(rows[b].at[src, grp], dst, dn_zs.at[b, i], dn_zr.at[b, i], {"fs": peer(d)})

    def dn_x(b, i):
        block = dn[b].at[origin(1 + i // 2), dn_part(i), grp]
        return remote(block, block, dn_xs.at[b, i], dn_xr.at[b, i], partner)

    def dn_landed(b, i):
        d = 1 + i // 2
        block = dn[b].at[origin(d), dn_part(i), grp]
        return remote(block, block, dn_zs.at[b, i], dn_zr.at[b, i], {"fs": origin(d)})

    gu_list = [("gu", i) for i in range((n_fs - 1) * base)]
    dn_list = [("dn", i) for i in range((n_fs - 1) * 2)]

    def piece(kind, i):
        if kind == "gu":
            return gu_z, gu_landed, gu_x, gu_cond, 1 + i // base
        return dn_z, dn_landed, dn_x, dn_cond, 1 + i // 2

    def issue(b, pieces):
        for kind, i in pieces:
            along_z, _, _, cond, d = piece(kind, i)
            when(cond(i, peer(d)), lambda: along_z(b, i).start())

    def forward(b, pieces):
        for kind, i in pieces:
            _, landed, along_x, cond, _ = piece(kind, i)

            def go():
                landed(b, i).wait_recv()
                along_x(b, i).start()

            when(cond(i, fs), go)

    def collect(b, pieces):
        for kind, i in pieces:
            _, _, along_x, cond, _ = piece(kind, i)
            when(cond(i, fs), lambda: along_x(b, i).wait_recv())

    def drain(b, pieces):
        for kind, i in pieces:
            along_z, _, along_x, cond, d = piece(kind, i)
            when(cond(i, peer(d)), lambda: along_z(b, i).wait_send())
            when(cond(i, fs), lambda: along_x(b, i).wait_send())

    def load(b, m):
        dst = (wide_gate, wide_up, wide_down)[m]
        return pltpu.make_async_copy(weights[3 * b + m], dst, load_sem.at[m])

    def cast_columns(b):
        load(b, 0).wait()
        load(b, 1).wait()
        half, step = cols[b].shape[2], 32
        for h in range(2):

            def one(r, carry):
                at = pl.ds(pl.multiple_of(h * half + r * step, step), step)
                to = pl.ds(pl.multiple_of(r * step, step), step)
                for t in range(tiles):
                    lane = pl.ds(t * LANES, LANES)
                    cols[b][t, h, to, :LANES] = wide_gate[at, lane].astype(bf)
                    cols[b][t, h, to, LANES:] = wide_up[at, lane].astype(bf)
                return carry

            lax.fori_loop(0, half // step, one, 0)
        own_tiles(cols[b], lambda n: gu[b].at[n, fs])

    def cast_rows(b):
        load(b, 2).wait()
        half = rows[b].shape[2]

        def one(i, carry):
            at = pl.ds(pl.multiple_of(i * half, half), half)
            rows[b][lax.div(i, 2), lax.rem(i, 2)] = wide_down[at, :].astype(bf)
            return carry

        lax.fori_loop(0, 2 * tiles, one, 0)
        own_tiles(rows[b], lambda n: dn[b].at[fs, n])

    def own_tiles(src, dst):
        start = first_tile(fs)
        for n in range(base):
            def copy():
                dst(n)[...] = src[start + n]

            if n < base - 1 or not short:
                copy()
            else:
                pl.when(has_last(fs))(copy)

    def blank_tiles(b):
        if short:
            @pl.when(jnp.logical_not(has_last(fs)))
            def _():
                gu[b][base - 1] = jnp.zeros(gu[b].shape[1:], bf)
                for a in range(n_fs):
                    dn[b][a, base - 1] = jnp.zeros(dn[b].shape[2:], bf)

    def ag_right(b, o):
        block = x[b].at[tp, o]
        return remote(block, block, ag_zs.at[b, 0, o], ag_zr.at[b, o], {"fs": peer(1)})

    def ag_left(b, o):
        block = x[b].at[tp, o]
        return remote(block, block, ag_zs.at[b, 1, o], ag_zr.at[b, o], {"fs": origin(1)})

    def ag_y(b, o, mine=True):
        block = x[b].at[tp if mine else far_tp, o]
        return remote(block, block, ag_ys.at[b, o], ag_yr.at[b, o], across)

    def ag_core(b, o, j):
        block = x[b].at[far_tp if j else tp, o]
        return remote(block, block, ag_cs.at[b, j, o], ag_cr.at[b, j, o], other_core)

    def ag_own(b):
        pl.when(fs < last)(lambda: ag_right(b, fs).start())
        pl.when(fs > 0)(lambda: ag_left(b, fs).start())
        ag_y(b, fs).start()
        ag_core(b, fs, 0).start()

    def ag_hop(b, h):
        @pl.when(fs - 1 - h >= 0)
        def _():
            o = fs - 1 - h
            ag_right(b, o).wait_recv()
            pl.when(fs < last)(lambda: ag_right(b, o).start())
            ag_y(b, o).start()
            ag_core(b, o, 0).start()

        @pl.when(fs + 1 + h <= last)
        def _():
            o = fs + 1 + h
            ag_left(b, o).wait_recv()
            pl.when(fs > 0)(lambda: ag_left(b, o).start())
            ag_y(b, o).start()
            ag_core(b, o, 0).start()

    def ag_share(b, o):
        ag_y(b, o, False).wait_recv()
        ag_core(b, o, 1).start()

    def ag_share_hop(b, h):
        pl.when(fs - 1 - h >= 0)(lambda: ag_share(b, fs - 1 - h))
        pl.when(fs + 1 + h <= last)(lambda: ag_share(b, fs + 1 + h))

    def ag_finish(b):
        for o in range(n_fs):
            for j in range(2):
                ag_core(b, o, j).wait_recv()

    def ag_drain(b):
        for o in range(n_fs):
            if o < last:
                pl.when((fs < last) & (fs >= o))(lambda: ag_right(b, o).wait_send())
            if o > 0:
                pl.when((fs > 0) & (fs <= o))(lambda: ag_left(b, o).wait_send())
            ag_y(b, o).wait_send()
            for j in range(2):
                ag_core(b, o, j).wait_send()

    def norm(b):
        count, step = x[b].shape[2], 64
        width = x[b].shape[3]
        per = count // step

        def one(i, carry):
            k, at = lax.div(i, per), pl.ds(pl.multiple_of(lax.rem(i, per) * step, step), step)
            squares = jnp.zeros((step, width), f32)
            for t in range(n_tp):
                v = x[b][t, k, at, :].astype(f32)
                squares = squares + v * v
            mean = jnp.sum(squares, axis=1, keepdims=True) / (width * n_tp)
            factor = lax.rsqrt(mean + epsilon)
            for t in range(n_tp):
                v = x[b][t, k, at, :].astype(f32) * factor * all_gains[t, b : b + 1, :]
                normed[k, at, t * width : (t + 1) * width] = v.astype(bf)
            return carry

        lax.fori_loop(0, n_fs * per, one, 0)

    def make_hidden(b):
        start = first_tile(fs)

        def one(k, carry):
            for n in range(base):
                part = gu[b][n].reshape(-1, 2 * LANES)
                both = jnp.dot(normed[k], part, preferred_element_type=f32)
                gate = both[:, :LANES] * scales[2 * b, start + n]
                up = both[:, LANES:] * scales[2 * b + 1, start + n]
                value = gate / (1.0 + jnp.exp(-gate)) * up
                hidden[k, :, n * LANES : (n + 1) * LANES] = value.astype(bf)
            return carry

        lax.fori_loop(0, n_fs, one, 0)

    def term(b, a, k):
        part = dn[b][a].reshape(-1, dn[b].shape[4])
        return jnp.dot(hidden[k], part, preferred_element_type=f32)

    def rs_core(b, j, k):
        return remote(core_out.at[j, k], from_core[b].at[j, k], rs_cs.at[b, j, k], rs_cr.at[b, j, k], other_core)

    def rs_y(b, k):
        return remote(y_out.at[k], from_y[b].at[k], rs_ys.at[b, k], rs_yr.at[b, k], across)

    def rs_right(b, k):
        return remote(z_out.at[k], from_left[b].at[k], rs_zs.at[b, k], rs_lr.at[b, k], {"fs": peer(1)})

    def rs_left(b, k):
        return remote(z_out.at[k], from_right[b].at[k], rs_zs.at[b, k], rs_rr.at[b, k], {"fs": origin(1)})

    def turn(kk):
        odd = lax.rem(kk, 2)
        k = (1 - odd) * (last - lax.div(kk, 2)) + odd * lax.div(kk, 2)
        flip = lax.div(2 * fs, n_fs)
        return k + flip * (last - 2 * k)

    def scatter(b, hook):
        for j in range(2):
            target = 2 * (1 - chip if j == 0 else chip) + 1 - core

            def one(kk, carry):
                k = turn(kk)
                core_out[j, k] = term(b, target, k).astype(bf)
                rs_core(b, j, k).start()
                return carry

            lax.fori_loop(0, n_fs, one, 0)
        hook("core")

        def two(kk, carry):
            k = turn(kk)
            value = term(b, far_tp, k)
            rs_core(b, 0, k).wait_recv()
            y_out[k] = (value + from_core[b][0, k].astype(f32)).astype(bf)
            rs_y(b, k).start()
            return carry

        lax.fori_loop(0, n_fs, two, 0)
        hook("y")
        for kk in range(n_fs):
            k = turn(kk)
            rs_core(b, 1, k).wait_recv()
            total[...] = term(b, tp, k) + from_core[b][1, k].astype(f32)
            rs_y(b, k).wait_recv()
            total[...] = total[...] + from_y[b][k].astype(f32)

            @pl.when((k > fs) & (fs > 0))
            def _():
                rs_right(b, k).wait_recv()
                total[...] = total[...] + from_left[b][k].astype(f32)

            @pl.when((k < fs) & (fs < last))
            def _():
                rs_left(b, k).wait_recv()
                total[...] = total[...] + from_right[b][k].astype(f32)

            @pl.when(k == fs)
            def _():
                kept[...] = total[...]

            @pl.when(k != fs)
            def _():
                z_out[k] = total[...].astype(bf)

            pl.when(k > fs)(lambda: rs_right(b, k).start())
            pl.when(k < fs)(lambda: rs_left(b, k).start())
            hook(kk)

        @pl.when(fs > 0)
        def _():
            rs_right(b, fs).wait_recv()
            kept[...] = kept[...] + from_left[b][fs].astype(f32)

        @pl.when(fs < last)
        def _():
            rs_left(b, fs).wait_recv()
            kept[...] = kept[...] + from_right[b][fs].astype(f32)

        value = x[b][tp, fs].astype(f32) + 0.5 * kept[...] * down_scales[b : b + 1, :]
        return value.astype(bf)

    def scatter_drain(b):
        for k in range(n_fs):
            for j in range(2):
                rs_core(b, j, k).wait_send()
            rs_y(b, k).wait_send()
            pl.when(fs < k)(lambda: rs_right(b, k).wait_send())
            pl.when(fs > k)(lambda: rs_left(b, k).wait_send())

    own_tokens = pltpu.make_async_copy(tokens, x[0].at[tp, fs], load_sem.at[3])
    own_tokens.start()
    for m in range(3):
        load(0, m).start()

    barrier = pltpu.get_barrier_semaphore()
    greeted = [{"fs": peer(d)} for d in range(1, n_fs)] + [partner]
    greeted = greeted + [{"tp": lax.rem(tp + r, n_tp)} for r in range(1, n_tp)]
    for device in greeted:
        pl.semaphore_signal(barrier, inc=1, device_id=device, device_id_type=MESH)
    pl.semaphore_wait(barrier, len(greeted))

    def gain_copy(r):
        return remote(
            gains, all_gains.at[tp], gain_send.at[r - 1], gain_recv.at[r - 1], {"tp": lax.rem(tp + r, n_tp)}
        )

    own_tokens.wait()
    ag_own(0)
    for r in range(1, n_tp):
        gain_copy(r).start()
    all_gains[tp] = gains[...]
    for b in range(2):
        blank_tiles(b)
    cast_columns(0)
    load(1, 0).start()
    load(1, 1).start()
    issue(0, gu_list[:2])
    ag_hop(0, 0)
    issue(0, gu_list[2:4])
    ag_share(0, fs)
    ag_hop(0, 1)
    issue(0, gu_list[4:6])
    ag_share_hop(0, 0)
    for h in range(2, last):
        ag_hop(0, h)
    issue(0, gu_list[6:])
    cast_rows(0)
    load(1, 2).start()
    issue(0, dn_list)
    cut = len(gu_list) // 3
    forward(0, gu_list[:cut])
    for h in range(1, last):
        ag_share_hop(0, h)
    cast_columns(1)
    forward(0, gu_list[cut : 2 * cut])
    cast_rows(1)
    ag_finish(0)
    for r in range(1, n_tp):
        gain_copy(r).wait_recv()
    norm(0)
    forward(0, gu_list[2 * cut :])
    collect(0, gu_list)
    make_hidden(0)
    every = gu_list + dn_list
    issue(1, every[:5])
    forward(0, dn_list)
    collect(0, dn_list)

    def hook(stage):
        if stage == 0:
            forward(1, every[0:2])
            issue(1, every[5:7])
        if stage == 1:
            forward(1, every[2:4])
            issue(1, every[7:8])
        if stage == 2:
            forward(1, every[4:6])
            issue(1, every[8:9])
        if stage == 3:
            issue(1, every[9:10])

    x[1][tp, fs] = scatter(0, hook)
    ag_own(1)
    issue(1, every[10:11])
    forward(1, every[6:8])
    ag_hop(1, 0)
    issue(1, every[11:12])
    ag_share(1, fs)
    forward(1, every[8:9])
    ag_hop(1, 1)
    issue(1, every[12:13])
    ag_share_hop(1, 0)
    forward(1, every[9:10])
    for h in range(2, last):
        ag_hop(1, h)
    issue(1, every[13:])
    for h in range(1, last):
        ag_share_hop(1, h)
        forward(1, every[9 + h : 10 + h])
    forward(1, every[9 + last :])
    scatter_drain(0)
    ag_finish(1)
    norm(1)
    collect(1, gu_list)
    make_hidden(1)
    collect(1, dn_list)
    out[...] = scatter(1, lambda stage: None)
    scatter_drain(1)
    for b in range(2):
        ag_drain(b)
        drain(b, every)
    for r in range(1, n_tp):
        gain_copy(r).wait_send()


def body_kernel(tokens, *rest):
    first, second = rest[:7], rest[7:]
    n_fs, n_tp = lax.axis_size("fs"), lax.axis_size("tp")
    count, feats = tokens.shape
    depth, units = first[1].shape
    tiles = units // LANES
    base = -(-tiles // n_fs)
    half = depth // 2
    bf, f32 = jnp.bfloat16, jnp.float32
    gains = jnp.stack([first[0], second[0]])
    scales = jnp.stack([first[2], first[4], second[2], second[4]]).reshape(4, tiles, 1, LANES)
    scales = jnp.pad(scales, ((0, 0), (0, base), (0, 0), (0, 0)))
    down_scales = jnp.stack([first[6], second[6]])
    weights = [first[1], first[3], first[5], second[1], second[3], second[5]]
    vmem, dma = pltpu.VMEM, pltpu.SemaphoreType.DMA
    any_spec, vmem_spec = pl.BlockSpec(memory_space=pl.ANY), pl.BlockSpec(memory_space=pltpu.VMEM)
    tile = (count, feats)
    scratch = [
        vmem((depth, units), f32), vmem((depth, units), f32), vmem((units, feats), f32),
        vmem((n_tp, 2, feats), f32),
    ]
    scratch += [vmem((tiles, 2, half, 2 * LANES), bf)] * 2
    scratch += [vmem((tiles, 2, LANES // 2, feats), bf)] * 2
    scratch += [vmem((base, n_fs, 2, half, 2 * LANES), bf)] * 2
    scratch += [vmem((n_fs, base, 2, LANES // 2, feats), bf)] * 2
    scratch += [vmem((n_tp, n_fs, *tile), bf)] * 2
    scratch += [vmem((n_fs, count, n_tp * feats), bf), vmem((n_fs, count, base * LANES), bf)]
    scratch += [vmem((2, n_fs, *tile), bf)] * 3
    scratch += [vmem((n_fs, *tile), bf)] * 3
    scratch += [vmem((n_fs, *tile), bf)] * 5
    scratch += [vmem(tile, f32)] * 2
    scratch += [dma((4,)), dma((n_tp - 1,)), dma((n_tp - 1,))]
    scratch += [dma((2, 2, n_fs)), dma((2, n_fs)), dma((2, n_fs)), dma((2, n_fs)), dma((2, 2, n_fs)), dma((2, 2, n_fs))]
    scratch += [dma((2, (n_fs - 1) * base))] * 4 + [dma((2, (n_fs - 1) * 2))] * 4
    scratch += [dma((2, 2, n_fs))] * 2 + [dma((2, n_fs))] * 5
    return pl.pallas_call(
        functools.partial(both_blocks, n_fs, n_tp, tiles),
        out_shape=jax.ShapeDtypeStruct(tile, bf),
        in_specs=[any_spec] + [vmem_spec] * 3 + [any_spec] * 6,
        out_specs=vmem_spec,
        scratch_shapes=scratch,
        compiler_params=pltpu.CompilerParams(
            collective_id=0, has_side_effects=True, vmem_limit_bytes=67043328
        ),
    )(tokens, gains, scales, down_scales, *weights)


def fits(tokens, *rest):
    n_grp, n_fs, n_tp = (lax.axis_size(name) for name in ("grp", "fs", "tp"))
    depth, units = rest[1].shape
    return (
        n_grp == 2
        and n_fs == n_tp
        and n_tp == 4
        and units % LANES == 0
        and units // LANES > n_fs
        and depth % 64 == 0
        and depth == tokens.shape[1]
        and depth % LANES == 0
        and tokens.shape[0] % 64 == 0
    )


def solution(mesh):
    in_specs = (
        P(("grp", "fs"), "tp"),
        P("tp"),
        P("fs", "tp"),
        P("tp"),
        P("fs", "tp"),
        P("tp"),
        P("tp", "fs"),
        P("tp"),
        P("tp"),
        P("fs", "tp"),
        P("tp"),
        P("fs", "tp"),
        P("tp"),
        P("tp", "fs"),
        P("tp"),
    )
    out_specs = P(("grp", "fs"), "tp")

    def body(*args):
        return (body_kernel if fits(*args) else body_gather)(*args)

    return jax.shard_map(body, mesh=mesh, in_specs=in_specs, out_specs=out_specs, check_vma=False)
```

profile of v0, /device:TPU:0, one launch (start us, length us, event | category | flops | bytes accessed | tf_op | source)
XLA Modules:
  0.0 221.6 jit_solution(12562650232750170926)
XLA Ops:
  0.0 0.7 stack.36
  0.7 0.7 stack.37
  1.4 0.7 stack.38
  2.1 0.7 stack.39
  2.8 0.6 select_maximum_fusion.refs_2_
  3.5 1.3 pad_maximum_fusion
  4.8 215.1 %shard_map.145 = bf16[256,512]{1,0:T(8,128)(2,1)} custom-call(bf16[256,512]{1,0:T(8,128)(2,1)} %refs_0_.1, f32[2,512]{1,0:T(2,128)} %get-tuple-element.5.refs_1_, f32[4,14,1,128]{3,2,1,0:T(1,128)} %select_maximum_fusion.refs_2_, f32[2,512]{1,0:T(2,128)} %get-tuple-element.6.refs_3_, f32[512,1408]{1,0:T(8,128)} %refs_4_.1, f32[512,1408]{1,0:T(8,128)} %refs_5_.1, ...), custom_call_target="tpu_custom_call" | custom-call | tf_op jit(solution)/shard_map/pallas_call | solution.py:554
  220.0 1.7 copy.17
where the time goes:
time: 222 us
  Pallas kernels  215 us (97%)
  local copies, waits for them, and re-layouts  4.5 us (2%)
    pallas_call x1, Pallas kernels, body_kernel(): pl.pallas_call(functools.partial(both_blocks, n_fs, n_tp, tiles), out_sha...  215 us

commit v1 on v0

v1 whole, which is shorter than its diff:
```python
import functools

import jax
import jax.numpy as jnp
from jax import lax
from jax.experimental import pallas as pl
from jax.experimental.pallas import tpu as pltpu
from jax.sharding import PartitionSpec as P

MESH = pl.DeviceIdType.MESH
LANES = 128
PARTS = 2

epsilon = 1e-06


def normalize(stream, gain):
    values = stream.astype(jnp.float32)
    totals = lax.psum(jnp.sum(values * values, axis=1), "tp")
    width = values.shape[1] * lax.axis_size("tp")
    normed = (values * lax.rsqrt(totals / width + epsilon)[:, None] * gain).astype(jnp.bfloat16)
    return values, lax.all_gather(normed, "tp", axis=1, tiled=True)


def gathered_block(stream, gain, gate_w, gate_s, up_w, up_s, down_w, down_s):
    values, whole = normalize(stream, gain)

    def project(weight, scale):
        rows = lax.all_gather(weight.astype(jnp.bfloat16), "fs", axis=0, tiled=True)
        return jnp.dot(whole, rows, preferred_element_type=jnp.float32) * scale

    hidden = (jax.nn.silu(project(gate_w, gate_s)) * project(up_w, up_s)).astype(jnp.bfloat16)
    columns = lax.all_gather(down_w.astype(jnp.bfloat16), "fs", axis=1, tiled=True)
    terms = jnp.dot(hidden, columns, preferred_element_type=jnp.float32).astype(jnp.bfloat16)
    summed = lax.psum_scatter(terms, "tp", scatter_dimension=1, tiled=True).astype(jnp.float32)
    return (values + 0.5 * summed * down_s).astype(jnp.bfloat16)


def body_gather(tokens, *rest):
    middle = gathered_block(tokens, *rest[:7])
    return gathered_block(middle, *rest[7:])


def both_blocks(n_fs, n_tp, tiles, parts, *refs):
    tokens, small, weights, out, refs = refs[0], refs[1:9], refs[9:15], refs[15], refs[16:]
    (
        wide_gate, wide_up, wide_down, gains, all_gains, scales, down_scales,
        cols_0, cols_1, rows_0, rows_1, gu_0, gu_1, dn_0, dn_1, x_0, x_1, normed, hidden,
        core_out, from_core_0, from_core_1, y_out, from_y_0, from_y_1,
        z_out, from_left_0, from_left_1, from_right_0, from_right_1, total, kept,
        load_sem, small_sem, gain_send, gain_recv,
        ag_zs, ag_zr, ag_ys, ag_yr, ag_cs, ag_cr,
        gu_zs, gu_zr, gu_xs, gu_xr, dn_zs, dn_zr, dn_xs, dn_xr,
        rs_cs, rs_cr, rs_ys, rs_yr, rs_zs, rs_lr, rs_rr,
    ) = refs
    cols, rows, gu, dn, x = (cols_0, cols_1), (rows_0, rows_1), (gu_0, gu_1), (dn_0, dn_1), (x_0, x_1)
    from_core, from_y = (from_core_0, from_core_1), (from_y_0, from_y_1)
    from_left, from_right = (from_left_0, from_left_1), (from_right_0, from_right_1)

    grp, fs, tp = lax.axis_index("grp"), lax.axis_index("fs"), lax.axis_index("tp")
    core, chip = lax.rem(tp, 2), lax.div(tp, 2)
    partner, other_core, across = {"grp": 1 - grp}, {"tp": tp + 1 - 2 * core}, {"tp": lax.rem(tp + 2, n_tp)}
    far_tp = lax.rem(tp + 2, n_tp)
    last = n_fs - 1
    base = -(-tiles // n_fs)
    short = n_fs * base - tiles
    bf, f32 = jnp.bfloat16, jnp.float32

    def first_tile(dev):
        even = jnp.minimum(dev, short)
        odd = jnp.maximum(dev - (n_fs - short), 0)
        return dev * base - (1 - core) * even - core * odd

    def has_last(dev):
        return first_tile(dev + 1) - first_tile(dev) == base

    def peer(d):
        return lax.rem(fs + d, n_fs)

    def other(j):
        flip = lax.div(2 * fs, n_fs)
        place = fs + flip * (last - 2 * fs)
        o = j + jnp.where(place <= j, 1, 0)
        return o + flip * (last - 2 * o)

    def remote(src, dst, sends, recvs, device):
        return pltpu.make_async_remote_copy(
            src_ref=src, dst_ref=dst, send_sem=sends, recv_sem=recvs, device_id=device, device_id_type=MESH
        )

    def when(cond, fn):
        if cond is None:
            fn()
        else:
            pl.when(cond)(fn)

    def gu_cond(i, dev):
        return has_last(dev) if i // last == base - 1 and short else None

    def gu_z(b, i):
        to, n = other(i % last), i // last
        src = cols[b].at[first_tile(to) + n, grp]
        return remote(src, gu[b].at[n, fs, grp], gu_zs.at[b, i], gu_zr.at[b, n, fs], {"fs": to})

    def gu_landed(b, i):
        o, n = other(i % last), i // last
        block = gu[b].at[n, o, grp]
        return remote(block, block, gu_zs.at[b, i], gu_zr.at[b, n, o], {"fs": o})

    def gu_x(b, i):
        block = gu[b].at[i // last, other(i % last), grp]
        return remote(block, block, gu_xs.at[b, i], gu_xr.at[b, i], partner)

    def dn_part(i):
        return pl.ds(0, base - 1) if i < last else pl.ds(base - 1, 1)

    def dn_cond(i, dev):
        return has_last(dev) if i >= last and short else None

    def dn_z(b, i):
        to = other(i % last)
        start = first_tile(to)
        src = pl.ds(start, base - 1) if i < last else pl.ds(start + base - 1, 1)
        dst = dn[b].at[fs, dn_part(i), grp]
        return remote(rows[b].at[src, grp], dst, dn_zs.at[b, i], dn_zr.at[b, i // last, fs], {"fs": to})

    def dn_landed(b, i):
        o = other(i % last)
        block = dn[b].at[o, dn_part(i), grp]
        return remote(block, block, dn_zs.at[b, i], dn_zr.at[b, i // last, o], {"fs": o})

    def dn_x(b, i):
        block = dn[b].at[other(i % last), dn_part(i), grp]
        return remote(block, block, dn_xs.at[b, i], dn_xr.at[b, i], partner)

    gu_list = [("gu", i) for i in range((n_fs - 1) * base)]
    dn_list = [("dn", i) for i in range((n_fs - 1) * 2)]

    def piece(kind, i):
        if kind == "gu":
            return gu_z, gu_landed, gu_x, gu_cond, i % last
        return dn_z, dn_landed, dn_x, dn_cond, i % last

    def issue(b, pieces):
        for kind, i in pieces:
            along_z, _, _, cond, j = piece(kind, i)
            when(cond(i, other(j)), lambda: along_z(b, i).start())

    def forward(b, pieces):
        for kind, i in pieces:
            _, landed, along_x, cond, _ = piece(kind, i)

            def go():
                landed(b, i).wait_recv()
                along_x(b, i).start()

            when(cond(i, fs), go)

    def collect(b, pieces):
        for kind, i in pieces:
            _, _, along_x, cond, _ = piece(kind, i)
            when(cond(i, fs), lambda: along_x(b, i).wait_recv())

    def drain(b, pieces):
        for kind, i in pieces:
            along_z, _, along_x, cond, j = piece(kind, i)
            when(cond(i, other(j)), lambda: along_z(b, i).wait_send())
            when(cond(i, fs), lambda: along_x(b, i).wait_send())

    def load(b, m):
        dst = (wide_gate, wide_up, wide_down)[m]
        return pltpu.make_async_copy(weights[3 * b + m], dst, load_sem.at[m])

    def cast_columns(b):
        load(b, 0).wait()
        load(b, 1).wait()
        half, step = cols[b].shape[2], 32
        for h in range(2):

            def one(r, carry):
                at = pl.ds(pl.multiple_of(h * half + r * step, step), step)
                to = pl.ds(pl.multiple_of(r * step, step), step)
                for t in range(tiles):
                    lane = pl.ds(t * LANES, LANES)
                    cols[b][t, h, to, :LANES] = wide_gate[at, lane].astype(bf)
                    cols[b][t, h, to, LANES:] = wide_up[at, lane].astype(bf)
                return carry

            lax.fori_loop(0, half // step, one, 0)
        own_tiles(cols[b], lambda n: gu[b].at[n, fs])

    def cast_rows(b):
        load(b, 2).wait()
        half = rows[b].shape[2]

        def one(i, carry):
            at = pl.ds(pl.multiple_of(i * half, half), half)
            rows[b][lax.div(i, 2), lax.rem(i, 2)] = wide_down[at, :].astype(bf)
            return carry

        lax.fori_loop(0, 2 * tiles, one, 0)
        own_tiles(rows[b], lambda n: dn[b].at[fs, n])

    def own_tiles(src, dst):
        start = first_tile(fs)
        for n in range(base):
            def copy():
                dst(n)[...] = src[start + n]

            if n < base - 1 or not short:
                copy()
            else:
                pl.when(has_last(fs))(copy)

    def blank_tiles(b):
        if short:
            @pl.when(jnp.logical_not(has_last(fs)))
            def _():
                gu[b][base - 1] = jnp.zeros(gu[b].shape[1:], bf)
                for a in range(n_fs):
                    dn[b][a, base - 1] = jnp.zeros(dn[b].shape[2:], bf)

    def part(q):
        rows_q = x[0].shape[2] // parts
        return pl.ds(q * rows_q, rows_q)

    def ag_right(b, o, q):
        block = x[b].at[tp, o, part(q)]
        return remote(block, block, ag_zs.at[b, 0, o, q], ag_zr.at[b, o, q], {"fs": peer(1)})

    def ag_left(b, o, q):
        block = x[b].at[tp, o, part(q)]
        return remote(block, block, ag_zs.at[b, 1, o, q], ag_zr.at[b, o, q], {"fs": peer(last)})

    def ag_y(b, o, q, mine=True):
        block = x[b].at[tp if mine else far_tp, o, part(q)]
        return remote(block, block, ag_ys.at[b, o, q], ag_yr.at[b, o, q], across)

    def ag_core(b, o, q, j):
        block = x[b].at[far_tp if j else tp, o, part(q)]
        return remote(block, block, ag_cs.at[b, j, o, q], ag_cr.at[b, j, o, q], other_core)

    def ag_own(b, q):
        pl.when(fs < last)(lambda: ag_right(b, fs, q).start())
        pl.when(fs > 0)(lambda: ag_left(b, fs, q).start())
        ag_y(b, fs, q).start()
        ag_core(b, fs, q, 0).start()

    def ag_hop(b, h):
        for q in range(parts):
            @pl.when(fs - 1 - h >= 0)
            def _():
                o = fs - 1 - h
                ag_right(b, o, q).wait_recv()
                pl.when(fs < last)(lambda: ag_right(b, o, q).start())
                ag_y(b, o, q).start()
                ag_core(b, o, q, 0).start()

            @pl.when(fs + 1 + h <= last)
            def _():
                o = fs + 1 + h
                ag_left(b, o, q).wait_recv()
                pl.when(fs > 0)(lambda: ag_left(b, o, q).start())
                ag_y(b, o, q).start()
                ag_core(b, o, q, 0).start()

    def ag_share(b, o):
        for q in range(parts):
            ag_y(b, o, q, False).wait_recv()
            ag_core(b, o, q, 1).start()

    def ag_share_hop(b, h):
        pl.when(fs - 1 - h >= 0)(lambda: ag_share(b, fs - 1 - h))
        pl.when(fs + 1 + h <= last)(lambda: ag_share(b, fs + 1 + h))

    def ag_arrived(b, o):
        for q in range(parts):
            for j in range(2):
                ag_core(b, o, q, j).wait_recv()

    def ag_drain(b):
        for o in range(n_fs):
            for q in range(parts):
                if o < last:
                    pl.when((fs < last) & (fs >= o))(lambda: ag_right(b, o, q).wait_send())
                if o > 0:
                    pl.when((fs > 0) & (fs <= o))(lambda: ag_left(b, o, q).wait_send())
                ag_y(b, o, q).wait_send()
                for j in range(2):
                    ag_core(b, o, q, j).wait_send()

    def norm(b, k):
        step, width = 64, x[b].shape[3]

        def one(i, carry):
            at = pl.ds(pl.multiple_of(i * step, step), step)
            squares = jnp.zeros((step, width), f32)
            for t in range(n_tp):
                v = x[b][t, k, at, :].astype(f32)
                squares = squares + v * v
            mean = jnp.sum(squares, axis=1, keepdims=True) / (width * n_tp)
            factor = lax.rsqrt(mean + epsilon)
            for t in range(n_tp):
                v = x[b][t, k, at, :].astype(f32) * factor * all_gains[t, b]
                normed[k, at, t * width : (t + 1) * width] = v.astype(bf)
            return carry

        lax.fori_loop(0, x[b].shape[2] // step, one, 0)

    def make_hidden(b, k):
        for n in range(base):
            weight = gu[b][n].reshape(-1, 2 * LANES)
            both = jnp.dot(normed[k], weight, preferred_element_type=f32)
            gate = both[:, :LANES] * scales[2 * b, n]
            up = both[:, LANES:] * scales[2 * b + 1, n]
            value = gate / (1.0 + jnp.exp(-gate)) * up
            hidden[k, :, n * LANES : (n + 1) * LANES] = value.astype(bf)

    def every_block(fn):
        def one(k, carry):
            fn(k)
            return carry

        lax.fori_loop(0, n_fs, one, 0)

    def both_sides(h, fn):
        def one(side, carry):
            k = fs + (2 * side - 1) * (1 + h)
            pl.when((k >= 0) & (k <= last))(lambda: fn(k))
            return carry

        lax.fori_loop(0, 2, one, 0)

    def term(b, a, k):
        weight = dn[b][a].reshape(-1, dn[b].shape[4])
        return jnp.dot(hidden[k], weight, preferred_element_type=f32)

    def rs_core(b, j, k, q):
        src, dst = core_out.at[j, k, part(q)], from_core[b].at[j, k, part(q)]
        return remote(src, dst, rs_cs.at[b, j, k, q], rs_cr.at[b, j, k, q], other_core)

    def rs_y(b, k, q):
        src, dst = y_out.at[k, part(q)], from_y[b].at[k, part(q)]
        return remote(src, dst, rs_ys.at[b, k, q], rs_yr.at[b, k, q], across)

    def rs_right(b, k, q):
        src, dst = z_out.at[k, part(q)], from_left[b].at[k, part(q)]
        return remote(src, dst, rs_zs.at[b, k, q], rs_lr.at[b, k, q], {"fs": peer(1)})

    def rs_left(b, k, q):
        src, dst = z_out.at[k, part(q)], from_right[b].at[k, part(q)]
        return remote(src, dst, rs_zs.at[b, k, q], rs_rr.at[b, k, q], {"fs": peer(last)})

    def turn(kk):
        odd = lax.rem(kk, 2)
        k = (1 - odd) * (last - lax.div(kk, 2)) + odd * lax.div(kk, 2)
        flip = lax.div(2 * fs, n_fs)
        return k + flip * (last - 2 * k)

    def scatter(b, hook, finish):
        def to_core(j):
            target = 2 * (1 - chip if j == 0 else chip) + 1 - core

            def one(kk, carry):
                k = turn(kk)
                core_out[j, k] = term(b, target, k).astype(bf)
                for q in range(parts):
                    rs_core(b, j, k, q).start()
                return carry

            lax.fori_loop(0, n_fs, one, 0)

        def to_y(kk, carry):
            k = turn(kk)
            total[...] = term(b, far_tp, k)
            for q in range(parts):
                rs_core(b, 0, k, q).wait_recv()
                y_out[k, part(q)] = (total[part(q)] + from_core[b][0, k, part(q)].astype(f32)).astype(bf)
                rs_y(b, k, q).start()
            return carry

        to_core(0)
        hook("core")
        lax.fori_loop(0, n_fs, to_y, 0)
        to_core(1)
        hook("y")
        for kk in range(n_fs):
            k = turn(kk)
            total[...] = term(b, tp, k)
            for q in range(parts):
                at = part(q)
                rs_core(b, 1, k, q).wait_recv()
                rs_y(b, k, q).wait_recv()
                total[at] = total[at] + from_core[b][1, k, at].astype(f32) + from_y[b][k, at].astype(f32)

                @pl.when((k > fs) & (fs > 0))
                def _():
                    rs_right(b, k, q).wait_recv()
                    total[at] = total[at] + from_left[b][k, at].astype(f32)

                @pl.when((k < fs) & (fs < last))
                def _():
                    rs_left(b, k, q).wait_recv()
                    total[at] = total[at] + from_right[b][k, at].astype(f32)

                @pl.when(k == fs)
                def _():
                    kept[at] = total[at]

                @pl.when(k != fs)
                def _():
                    z_out[k, at] = total[at].astype(bf)

                pl.when(k > fs)(lambda: rs_right(b, k, q).start())
                pl.when(k < fs)(lambda: rs_left(b, k, q).start())
            hook(kk)

        for q in range(parts):
            at = part(q)

            @pl.when(fs > 0)
            def _():
                rs_right(b, fs, q).wait_recv()
                kept[at] = kept[at] + from_left[b][fs, at].astype(f32)

            @pl.when(fs < last)
            def _():
                rs_left(b, fs, q).wait_recv()
                kept[at] = kept[at] + from_right[b][fs, at].astype(f32)

            value = x[b][tp, fs, at].astype(f32) + 0.5 * kept[at] * down_scales[b]
            finish(q, value.astype(bf))

    def scatter_drain(b):
        for k in range(n_fs):
            for q in range(parts):
                for j in range(2):
                    rs_core(b, j, k, q).wait_send()
                rs_y(b, k, q).wait_send()
                pl.when(fs < k)(lambda: rs_right(b, k, q).wait_send())
                pl.when(fs > k)(lambda: rs_left(b, k, q).wait_send())

    own_tokens = pltpu.make_async_copy(tokens, x[0].at[tp, fs], load_sem.at[3])
    own_tokens.start()
    small_loads = []

    def small_load(src, dst):
        small_loads.append(pltpu.make_async_copy(src, dst, small_sem.at[len(small_loads)]))

    for b in range(2):
        gain, gate_s, up_s, down_s = small[4 * b : 4 * b + 4]
        small_load(gain, gains.at[b])
        small_load(down_s, down_scales.at[b])
        for n in range(base):
            at = pl.multiple_of(jnp.minimum(first_tile(fs) + n, tiles - 1) * LANES, LANES)
            for i, src in enumerate((gate_s, up_s)):
                small_load(src.at[:, pl.ds(at, LANES)], scales.at[2 * b + i, n])
    for copy in small_loads:
        copy.start()
    for m in range(3):
        load(0, m).start()

    barrier = pltpu.get_barrier_semaphore()
    greeted = [{"fs": peer(d)} for d in range(1, n_fs)] + [partner]
    greeted = greeted + [{"tp": lax.rem(tp + r, n_tp)} for r in range(1, n_tp)]
    for device in greeted:
        pl.semaphore_signal(barrier, inc=1, device_id=device, device_id_type=MESH)
    pl.semaphore_wait(barrier, len(greeted))

    def gain_copy(r):
        return remote(
            gains, all_gains.at[tp], gain_send.at[r - 1], gain_recv.at[r - 1], {"tp": lax.rem(tp + r, n_tp)}
        )

    own_tokens.wait()
    for q in range(parts):
        ag_own(0, q)
    for copy in small_loads:
        copy.wait()
    for r in range(1, n_tp):
        gain_copy(r).start()
    all_gains[tp] = gains[...]
    for b in range(2):
        blank_tiles(b)
    every = gu_list + dn_list
    count = len(gu_list)
    cast_columns(0)
    issue(0, every[:1])
    cast_rows(0)
    for m in range(3):
        load(1, m).start()
    ag_hop(0, 0)
    issue(0, every[1 : 2 * last])
    ag_share(0, fs)
    cast_columns(1)
    ag_hop(0, 1)
    issue(0, every[2 * last :])
    forward(0, every[:last])
    ag_share_hop(0, 0)
    cast_rows(1)
    forward(0, every[last : 2 * last])
    for h in range(2, last):
        ag_hop(0, h)
    ag_share_hop(0, 1)
    forward(0, every[2 * last : 3 * last - 1])
    for h in range(2, last):
        ag_share_hop(0, h)
    forward(0, every[3 * last - 1 : count])
    issue(1, every[:6])
    for r in range(1, n_tp):
        gain_copy(r).wait_recv()
    for o in range(n_fs):
        ag_arrived(0, o)
    every_block(lambda k: norm(0, k))
    forward(0, every[count : count + 2])
    collect(0, every[:count])
    every_block(lambda k: make_hidden(0, k))
    forward(0, every[count + 2 :])
    collect(0, every[count:])

    def hook(stage):
        if stage == "core":
            issue(1, every[6:8])
        if stage == 0:
            issue(1, every[8:9])
            forward(1, every[0:2])
        if stage == 1:
            issue(1, every[9:10])
            forward(1, every[2:3])
        if stage == 2:
            issue(1, every[10:11])
            forward(1, every[3:4])
        if stage == 3:
            forward(1, every[4:6])

    def pass_on(q, value):
        x[1][tp, fs, part(q)] = value
        ag_own(1, q)

    scatter(0, hook, pass_on)
    forward(1, every[6:7])
    ag_hop(1, 0)
    issue(1, every[11:13])
    ag_share(1, fs)
    forward(1, every[7:8])
    ag_hop(1, 1)
    issue(1, every[13:])
    ag_share_hop(1, 0)
    forward(1, every[8:9])
    ag_arrived(1, fs)
    norm(1, fs)
    for h in range(2, last):
        ag_hop(1, h)
    forward(1, every[9:10])

    def ready(k):
        ag_arrived(1, k)
        norm(1, k)

    for h in range(1, last):
        ag_share_hop(1, h)
        forward(1, every[9 + h : 10 + h])
        both_sides(h - 1, ready)
    forward(1, every[9 + last :])
    both_sides(last - 1, ready)
    collect(1, every[:count])
    every_block(lambda k: make_hidden(1, k))
    scatter_drain(0)
    collect(1, every[count:])

    def put_out(q, value):
        out[part(q)] = value

    scatter(1, lambda stage: None, put_out)
    scatter_drain(1)
    for b in range(2):
        ag_drain(b)
        drain(b, every)
    for r in range(1, n_tp):
        gain_copy(r).wait_send()


def body_kernel(tokens, *rest):
    first, second = rest[:7], rest[7:]
    n_fs, n_tp = lax.axis_size("fs"), lax.axis_size("tp")
    count, feats = tokens.shape
    depth, units = first[1].shape
    tiles = units // LANES
    base = -(-tiles // n_fs)
    half = depth // 2
    bf, f32 = jnp.bfloat16, jnp.float32
    small = []
    for gain, _, gate_s, _, up_s, _, down_s in (first, second):
        small += [gain[None, :], gate_s[None, :], up_s[None, :], down_s[None, :]]
    weights = [first[1], first[3], first[5], second[1], second[3], second[5]]
    vmem, dma = pltpu.VMEM, pltpu.SemaphoreType.DMA
    any_spec, vmem_spec = pl.BlockSpec(memory_space=pl.ANY), pl.BlockSpec(memory_space=pltpu.VMEM)
    tile = (count, feats)
    scratch = [
        vmem((depth, units), f32), vmem((depth, units), f32), vmem((units, feats), f32),
        vmem((2, 1, feats), f32), vmem((n_tp, 2, 1, feats), f32), vmem((4, base, 1, LANES), f32), vmem((2, 1, feats), f32),
    ]
    scratch += [vmem((tiles, 2, half, 2 * LANES), bf)] * 2
    scratch += [vmem((tiles, 2, LANES // 2, feats), bf)] * 2
    scratch += [vmem((base, n_fs, 2, half, 2 * LANES), bf)] * 2
    scratch += [vmem((n_fs, base, 2, LANES // 2, feats), bf)] * 2
    scratch += [vmem((n_tp, n_fs, *tile), bf)] * 2
    scratch += [vmem((n_fs, count, n_tp * feats), bf), vmem((n_fs, count, base * LANES), bf)]
    scratch += [vmem((2, n_fs, *tile), bf)] * 3
    scratch += [vmem((n_fs, *tile), bf)] * 3
    scratch += [vmem((n_fs, *tile), bf)] * 5
    scratch += [vmem(tile, f32)] * 2
    scratch += [dma((4,)), dma((4 + 4 * base,)), dma((n_tp - 1,)), dma((n_tp - 1,))]
    one, two = dma((2, n_fs, PARTS)), dma((2, 2, n_fs, PARTS))
    scratch += [two, one, one, one, two, two]
    for count_of in (base, 2):
        sent = dma((2, (n_fs - 1) * count_of))
        scratch += [sent, dma((2, count_of, n_fs)), sent, sent]
    scratch += [two] * 2 + [one] * 5
    return pl.pallas_call(
        functools.partial(both_blocks, n_fs, n_tp, tiles, PARTS),
        out_shape=jax.ShapeDtypeStruct(tile, bf),
        in_specs=[any_spec] * 15,
        out_specs=vmem_spec,
        scratch_shapes=scratch,
        compiler_params=pltpu.CompilerParams(
            collective_id=0, has_side_effects=True, vmem_limit_bytes=67043328
        ),
    )(tokens, *small, *weights)


def fits(tokens, *rest):
    n_grp, n_fs, n_tp = (lax.axis_size(name) for name in ("grp", "fs", "tp"))
    depth, units = rest[1].shape
    return (
        n_grp == 2
        and n_fs == n_tp
        and n_tp == 4
        and units % LANES == 0
        and units // LANES > n_fs
        and depth % 64 == 0
        and depth == tokens.shape[1]
        and depth % LANES == 0
        and tokens.shape[0] % 64 == 0
    )


def solution(mesh):
    in_specs = (
        P(("grp", "fs"), "tp"),
        P("tp"),
        P("fs", "tp"),
        P("tp"),
        P("fs", "tp"),
        P("tp"),
        P("tp", "fs"),
        P("tp"),
        P("tp"),
        P("fs", "tp"),
        P("tp"),
        P("fs", "tp"),
        P("tp"),
        P("tp", "fs"),
        P("tp"),
    )
    out_specs = P(("grp", "fs"), "tp")

    def body(*args):
        return (body_kernel if fits(*args) else body_gather)(*args)

    return jax.shard_map(body, mesh=mesh, in_specs=in_specs, out_specs=out_specs, check_vma=False)
```

time: 222 us -> 194 us (0.87)
  Pallas kernels: 215 us -> 187 us
  local copies, waits for them, and re-layouts: 4.5 us -> 6.85 us
    pallas_call x1, Pallas kernels: 215 us -> 187 us  [body_kernel(): pl.pallas_call(functools.partial(both_blocks, n_fs, n_tp, tiles, PARTS),...]
    broadcast_in_dim x0 -> x4, local copies, waits for them, and re-layouts: none -> 5.18 us  [body_kernel(): small += [gain[None, :], gate_s[None, :], up_s[None, :], down_s[None, :]]]
    another operation x4 -> x0, local copies, waits for them, and re-layouts: 2.83 us -> none  [body_kernel(): jnp.stack([first[2], first[4], second[2], second[4]])]
where the time goes in v1:
time: 194 us
  Pallas kernels  187 us (96%)
  local copies, waits for them, and re-layouts  6.85 us (4%)
    pallas_call x1, Pallas kernels, body_kernel(): pl.pallas_call(functools.partial(both_blocks, n_fs, n_tp, tiles, PARTS),...  187 us
    broadcast_in_dim x4, local copies, waits for them, and re-layouts, body_kernel(): small += [gain[None, :], gate_s[None, :], up_s[None, :], down_s[None, :]]  5.18 us

profile of v1, /device:TPU:0, one launch (start us, length us, event | category | flops | bytes accessed | tf_op | source)
XLA Modules:
  0.0 193.5 jit_solution(8196525881170464248)
XLA Ops:
  0.0 1.3 broadcast_in_dim.25.refs_2_
  1.3 1.3 broadcast_in_dim.26.refs_3_
  2.6 1.3 broadcast_in_dim.29.refs_6_
  3.9 1.3 broadcast_in_dim.30.refs_7_
  5.2 186.6 %shard_map.145 = bf16[256,512]{1,0:T(8,128)(2,1)} custom-call(bf16[256,512]{1,0:T(8,128)(2,1)} %refs_0_.1, f32[1,512]{1,0:T(1,128)} %bitcast.4, f32[1,1408]{1,0:T(1,128)} %broadcast_in_dim.25.refs_2_, f32[1,1408]{1,0:T(1,128)} %broadcast_in_dim.26.refs_3_, f32[1,512]{1,0:T(1,128)} %bitcast.5, f32[1,512]{1,0:T(1,128)} %bitcast.6, ...), custom_call_target="tpu_custom_call" | custom-call | tf_op jit(solution)/shard_map/pallas_call | solution.py:620
  191.8 1.7 copy.17

commit v2 on v1

--- a/solution.py
+++ b/solution.py
@@ -10,6 +10,18 @@
 MESH = pl.DeviceIdType.MESH
 LANES = 128
 PARTS = 2
+FIRST = 7
+PLAN = {
+    "core": (10, 0),
+    0: (11, 3),
+    1: (12, 5),
+    2: (13, 7),
+    3: (13, 9),
+    "own": (13, 10),
+    "hop0": (15, 12),
+    "hop1": (15, 13),
+    "hop2": (15, 15),
+}
 
 epsilon = 1e-06
 
@@ -44,7 +56,7 @@
 def both_blocks(n_fs, n_tp, tiles, parts, *refs):
     tokens, small, weights, out, refs = refs[0], refs[1:9], refs[9:15], refs[15], refs[16:]
     (
-        wide_gate, wide_up, wide_down, gains, all_gains, scales, down_scales,
+        wide_gate, wide_up, wide_down, gains, all_gains, scale_0, scale_1, scale_2, scale_3, down_scales,
         cols_0, cols_1, rows_0, rows_1, gu_0, gu_1, dn_0, dn_1, x_0, x_1, normed, hidden,
         core_out, from_core_0, from_core_1, y_out, from_y_0, from_y_1,
         z_out, from_left_0, from_left_1, from_right_0, from_right_1, total, kept,
@@ -53,6 +65,7 @@
         gu_zs, gu_zr, gu_xs, gu_xr, dn_zs, dn_zr, dn_xs, dn_xr,
         rs_cs, rs_cr, rs_ys, rs_yr, rs_zs, rs_lr, rs_rr,
     ) = refs
+    scales = (scale_0, scale_1, scale_2, scale_3)
     cols, rows, gu, dn, x = (cols_0, cols_1), (rows_0, rows_1), (gu_0, gu_1), (dn_0, dn_1), (x_0, x_1)
     from_core, from_y = (from_core_0, from_core_1), (from_y_0, from_y_1)
     from_left, from_right = (from_left_0, from_left_1), (from_right_0, from_right_1)
@@ -62,6 +75,7 @@
     partner, other_core, across = {"grp": 1 - grp}, {"tp": tp + 1 - 2 * core}, {"tp": lax.rem(tp + 2, n_tp)}
     far_tp = lax.rem(tp + 2, n_tp)
     last = n_fs - 1
+    at_end = (fs == 0) | (fs == last)
     base = -(-tiles // n_fs)
     short = n_fs * base - tiles
     bf, f32 = jnp.bfloat16, jnp.float32
@@ -307,12 +321,16 @@
 
         lax.fori_loop(0, x[b].shape[2] // step, one, 0)
 
+    def own_scale(i, n):
+        tile = jnp.minimum(first_tile(fs) + n, tiles - 1)
+        return scales[i][pl.ds(pl.multiple_of(tile * LANES, LANES), LANES)][None, :]
+
     def make_hidden(b, k):
         for n in range(base):
             weight = gu[b][n].reshape(-1, 2 * LANES)
             both = jnp.dot(normed[k], weight, preferred_element_type=f32)
-            gate = both[:, :LANES] * scales[2 * b, n]
-            up = both[:, LANES:] * scales[2 * b + 1, n]
+            gate = both[:, :LANES] * own_scale(2 * b, n)
+            up = both[:, LANES:] * own_scale(2 * b + 1, n)
             value = gate / (1.0 + jnp.exp(-gate)) * up
             hidden[k, :, n * LANES : (n + 1) * LANES] = value.astype(bf)
 
@@ -323,14 +341,6 @@
 
         lax.fori_loop(0, n_fs, one, 0)
 
-    def both_sides(h, fn):
-        def one(side, carry):
-            k = fs + (2 * side - 1) * (1 + h)
-            pl.when((k >= 0) & (k <= last))(lambda: fn(k))
-            return carry
-
-        lax.fori_loop(0, 2, one, 0)
-
     def term(b, a, k):
         weight = dn[b][a].reshape(-1, dn[b].shape[4])
         return jnp.dot(hidden[k], weight, preferred_element_type=f32)
@@ -352,71 +362,57 @@
         return remote(src, dst, rs_zs.at[b, k, q], rs_rr.at[b, k, q], {"fs": peer(last)})
 
     def turn(kk):
-        odd = lax.rem(kk, 2)
-        k = (1 - odd) * (last - lax.div(kk, 2)) + odd * lax.div(kk, 2)
         flip = lax.div(2 * fs, n_fs)
+        place = fs + flip * (last - 2 * fs)
+        odd, half = lax.rem(kk, 2), lax.div(kk, 2)
+        k = jnp.where(place == 0, last - kk, (1 - odd) * (last - half) + odd * half)
         return k + flip * (last - 2 * k)
 
-    def scatter(b, hook, finish):
-        def to_core(j):
-            target = 2 * (1 - chip if j == 0 else chip) + 1 - core
-
-            def one(kk, carry):
-                k = turn(kk)
-                core_out[j, k] = term(b, target, k).astype(bf)
-                for q in range(parts):
-                    rs_core(b, j, k, q).start()
-                return carry
-
-            lax.fori_loop(0, n_fs, one, 0)
-
-        def to_y(kk, carry):
-            k = turn(kk)
-            total[...] = term(b, far_tp, k)
-            for q in range(parts):
-                rs_core(b, 0, k, q).wait_recv()
-                y_out[k, part(q)] = (total[part(q)] + from_core[b][0, k, part(q)].astype(f32)).astype(bf)
-                rs_y(b, k, q).start()
-            return carry
-
-        to_core(0)
-        hook("core")
-        lax.fori_loop(0, n_fs, to_y, 0)
-        to_core(1)
-        hook("y")
-        for kk in range(n_fs):
-            k = turn(kk)
-            total[...] = term(b, tp, k)
-            for q in range(parts):
-                at = part(q)
-                rs_core(b, 1, k, q).wait_recv()
-                rs_y(b, k, q).wait_recv()
-                total[at] = total[at] + from_core[b][1, k, at].astype(f32) + from_y[b][k, at].astype(f32)
-
-                @pl.when((k > fs) & (fs > 0))
-                def _():
-                    rs_right(b, k, q).wait_recv()
-                    total[at] = total[at] + from_left[b][k, at].astype(f32)
-
-                @pl.when((k < fs) & (fs < last))
-                def _():
-                    rs_left(b, k, q).wait_recv()
-                    total[at] = total[at] + from_right[b][k, at].astype(f32)
-
-                @pl.when(k == fs)
-                def _():
-                    kept[at] = total[at]
-
-                @pl.when(k != fs)
-                def _():
-                    z_out[k, at] = total[at].astype(bf)
-
-                pl.when(k > fs)(lambda: rs_right(b, k, q).start())
-                pl.when(k < fs)(lambda: rs_left(b, k, q).start())
-            hook(kk)
-
+    def core_stage(b, j, k):
+        target = 2 * (1 - chip if j == 0 else chip) + 1 - core
+        core_out[j, k] = term(b, target, k).astype(bf)
+        for q in range(parts):
+            rs_core(b, j, k, q).start()
+
+    def y_stage(b, k):
+        total[...] = term(b, far_tp, k)
+        for q in range(parts):
+            rs_core(b, 0, k, q).wait_recv()
+            y_out[k, part(q)] = (total[part(q)] + from_core[b][0, k, part(q)].astype(f32)).astype(bf)
+            rs_y(b, k, q).start()
+
+    def z_stage(b, k):
+        total[...] = term(b, tp, k)
         for q in range(parts):
             at = part(q)
+            rs_core(b, 1, k, q).wait_recv()
+            rs_y(b, k, q).wait_recv()
+            total[at] = total[at] + from_core[b][1, k, at].astype(f32) + from_y[b][k, at].astype(f32)
+
+            @pl.when((k > fs) & (fs > 0))
+            def _():
+                rs_right(b, k, q).wait_recv()
+                total[at] = total[at] + from_left[b][k, at].astype(f32)
+
+            @pl.when((k < fs) & (fs < last))
+            def _():
+                rs_left(b, k, q).wait_recv()
+                total[at] = total[at] + from_right[b][k, at].astype(f32)
+
+            @pl.when(k == fs)
+            def _():
+                kept[at] = total[at]
+
+            @pl.when(k != fs)
+            def _():
+                z_out[k, at] = total[at].astype(bf)
+
+            pl.when(k > fs)(lambda: rs_right(b, k, q).start())
+            pl.when(k < fs)(lambda: rs_left(b, k, q).start())
+
+    def z_last(b, finish):
+        for q in range(parts):
+            at = part(q)
 
             @pl.when(fs > 0)
             def _():
@@ -430,6 +426,23 @@
 
             value = x[b][tp, fs, at].astype(f32) + 0.5 * kept[at] * down_scales[b]
             finish(q, value.astype(bf))
+
+    def loop(count, fn):
+        def one(i, carry):
+            fn(i)
+            return carry
+
+        lax.fori_loop(0, count, one, 0)
+
+    def scatter(b, hook, finish):
+        loop(n_fs, lambda i: core_stage(b, 0, turn(i)))
+        hook("core")
+        loop(n_fs, lambda i: y_stage(b, turn(i)))
+        loop(n_fs, lambda i: core_stage(b, 1, turn(i)))
+        for kk in range(n_fs):
+            z_stage(b, turn(kk))
+            hook(kk)
+        z_last(b, finish)
 
     def scatter_drain(b):
         for k in range(n_fs):
@@ -451,10 +464,8 @@
         gain, gate_s, up_s, down_s = small[4 * b : 4 * b + 4]
         small_load(gain, gains.at[b])
         small_load(down_s, down_scales.at[b])
-        for n in range(base):
-            at = pl.multiple_of(jnp.minimum(first_tile(fs) + n, tiles - 1) * LANES, LANES)
-            for i, src in enumerate((gate_s, up_s)):
-                small_load(src.at[:, pl.ds(at, LANES)], scales.at[2 * b + i, n])
+        small_load(gate_s, scales[2 * b])
+        small_load(up_s, scales[2 * b + 1])
     for copy in small_loads:
         copy.start()
     for m in range(3):
@@ -506,66 +517,61 @@
     for h in range(2, last):
         ag_share_hop(0, h)
     forward(0, every[3 * last - 1 : count])
-    issue(1, every[:6])
+    pl.when(at_end)(lambda: issue(1, every[:FIRST]))
     for r in range(1, n_tp):
         gain_copy(r).wait_recv()
     for o in range(n_fs):
         ag_arrived(0, o)
     every_block(lambda k: norm(0, k))
-    forward(0, every[count : count + 2])
+    forward(0, every[count : count + 1])
     collect(0, every[:count])
-    every_block(lambda k: make_hidden(0, k))
-    forward(0, every[count + 2 :])
+    for k in range(n_fs):
+        make_hidden(0, k)
+        forward(0, every[count + 1 + k : count + 2 + k])
+    forward(0, every[count + 1 + n_fs :])
+    pl.when(jnp.logical_not(at_end))(lambda: issue(1, every[:FIRST]))
     collect(0, every[count:])
 
+    sent, passed = [FIRST], [0]
+
     def hook(stage):
-        if stage == "core":
-            issue(1, every[6:8])
-        if stage == 0:
-            issue(1, every[8:9])
-            forward(1, every[0:2])
-        if stage == 1:
-            issue(1, every[9:10])
-            forward(1, every[2:3])
-        if stage == 2:
-            issue(1, every[10:11])
-            forward(1, every[3:4])
-        if stage == 3:
-            forward(1, every[4:6])
+        to_send, to_pass = PLAN.get(stage, (0, 0))
+        issue(1, every[sent[0] : to_send])
+        sent[0] = max(sent[0], to_send)
+        forward(1, every[passed[0] : to_pass])
+        passed[0] = max(passed[0], to_pass)
 
     def pass_on(q, value):
         x[1][tp, fs, part(q)] = value
         ag_own(1, q)
 
-    scatter(0, hook, pass_on)
-    forward(1, every[6:7])
-    ag_hop(1, 0)
-    issue(1, every[11:13])
-    ag_share(1, fs)
-    forward(1, every[7:8])
-    ag_hop(1, 1)
-    issue(1, every[13:])
-    ag_share_hop(1, 0)
-    forward(1, every[8:9])
-    ag_arrived(1, fs)
-    norm(1, fs)
-    for h in range(2, last):
-        ag_hop(1, h)
-    forward(1, every[9:10])
-
     def ready(k):
         ag_arrived(1, k)
         norm(1, k)
-
-    for h in range(1, last):
+        make_hidden(1, k)
+
+    scatter(0, hook, pass_on)
+    hook("own")
+    ag_hop(1, 0)
+    hook("hop0")
+    ag_share(1, fs)
+    ag_hop(1, 1)
+    hook("hop1")
+    ag_share_hop(1, 0)
+    collect(1, every[:count])
+    ready(fs)
+    for h in range(2, last):
+        ag_hop(1, h)
+        hook("hop%d" % h)
+    ag_share_hop(1, 1)
+    hook("share1")
+    loop(last - 1, lambda i: ready(other(i)))
+    scatter_drain(0)
+    issue(1, every[sent[0] :])
+    forward(1, every[passed[0] :])
+    for h in range(2, last):
         ag_share_hop(1, h)
-        forward(1, every[9 + h : 10 + h])
-        both_sides(h - 1, ready)
-    forward(1, every[9 + last :])
-    both_sides(last - 1, ready)
-    collect(1, every[:count])
-    every_block(lambda k: make_hidden(1, k))
-    scatter_drain(0)
+    ready(other(last - 1))
     collect(1, every[count:])
 
     def put_out(q, value):
@@ -591,14 +597,14 @@
     bf, f32 = jnp.bfloat16, jnp.float32
     small = []
     for gain, _, gate_s, _, up_s, _, down_s in (first, second):
-        small += [gain[None, :], gate_s[None, :], up_s[None, :], down_s[None, :]]
+        small += [gain[None, :], gate_s, up_s, down_s[None, :]]
     weights = [first[1], first[3], first[5], second[1], second[3], second[5]]
     vmem, dma = pltpu.VMEM, pltpu.SemaphoreType.DMA
     any_spec, vmem_spec = pl.BlockSpec(memory_space=pl.ANY), pl.BlockSpec(memory_space=pltpu.VMEM)
     tile = (count, feats)
     scratch = [
         vmem((depth, units), f32), vmem((depth, units), f32), vmem((units, feats), f32),
-        vmem((2, 1, feats), f32), vmem((n_tp, 2, 1, feats), f32), vmem((4, base, 1, LANES), f32), vmem((2, 1, feats), f32),
+        vmem((2, 1, feats), f32), vmem((n_tp, 2, 1, feats), f32), vmem((units,), f32), vmem((units,), f32), vmem((units,), f32), vmem((units,), f32), vmem((2, 1, feats), f32),
     ]
     scratch += [vmem((tiles, 2, half, 2 * LANES), bf)] * 2
     scratch += [vmem((tiles, 2, LANES // 2, feats), bf)] * 2
@@ -610,7 +616,7 @@
     scratch += [vmem((n_fs, *tile), bf)] * 3
     scratch += [vmem((n_fs, *tile), bf)] * 5
     scratch += [vmem(tile, f32)] * 2
-    scratch += [dma((4,)), dma((4 + 4 * base,)), dma((n_tp - 1,)), dma((n_tp - 1,))]
+    scratch += [dma((4,)), dma((8,)), dma((n_tp - 1,)), dma((n_tp - 1,))]
     one, two = dma((2, n_fs, PARTS)), dma((2, 2, n_fs, PARTS))
     scratch += [two, one, one, one, two, two]
     for count_of in (base, 2):

time: 194 us -> 176 us (0.907)
  Pallas kernels: 187 us -> 174 us
  local copies, waits for them, and re-layouts: 6.85 us -> 1.67 us
    pallas_call x1, Pallas kernels: 187 us -> 174 us  [body_kernel(): pl.pallas_call(functools.partial(both_blocks, n_fs, n_tp, tiles, PARTS),...]
    broadcast_in_dim x4 -> x0, local copies, waits for them, and re-layouts: 5.18 us -> none  [body_kernel(): small += [gain[None, :], gate_s[None, :], up_s[None, :], down_s[None, :]]]
where the time goes in v2:
time: 176 us; the launch traced here: 175 us
  Pallas kernels  174 us (99%)
    pallas_call x1, Pallas kernels, body_kernel(): pl.pallas_call(functools.partial(both_blocks, n_fs, n_tp, tiles, PARTS),...  174 us

profile of v2, /device:TPU:0, one launch (start us, length us, event | category | flops | bytes accessed | tf_op | source)
XLA Modules:
  0.0 175.5 jit_solution(16989291555123737638)
XLA Ops:
  0.0 173.8 %shard_map.145 = bf16[256,512]{1,0:T(8,128)(2,1)} custom-call(bf16[256,512]{1,0:T(8,128)(2,1)} %refs_0_.1, f32[1,512]{1,0:T(1,128)} %bitcast.4, f32[1408]{0:T(1024)} %refs_2_.1, f32[1408]{0:T(1024)} %refs_3_.1, f32[1,512]{1,0:T(1,128)} %bitcast.5, f32[1,512]{1,0:T(1,128)} %bitcast.6, f32[1408]{0:T(1024)} %refs_6_.1, f32[1408]{0:T(1024)} %refs_7_.1, ...), custom_call_target="tpu_custom_call" | custom-call | tf_op jit(solution)/shard_map/pallas_call | solution.py:626
  173.8 1.7 copy.17

commit v3 on v2

--- a/solution.py
+++ b/solution.py
@@ -384,10 +384,12 @@
     def z_stage(b, k):
         total[...] = term(b, tp, k)
         for q in range(parts):
+            rs_core(b, 1, k, q).wait_recv()
+            total[part(q)] = total[part(q)] + from_core[b][1, k, part(q)].astype(f32)
+        for q in range(parts):
             at = part(q)
-            rs_core(b, 1, k, q).wait_recv()
             rs_y(b, k, q).wait_recv()
-            total[at] = total[at] + from_core[b][1, k, at].astype(f32) + from_y[b][k, at].astype(f32)
+            total[at] = total[at] + from_y[b][k, at].astype(f32)
 
             @pl.when((k > fs) & (fs > 0))
             def _():
@@ -435,9 +437,14 @@
         lax.fori_loop(0, count, one, 0)
 
     def scatter(b, hook, finish):
-        loop(n_fs, lambda i: core_stage(b, 0, turn(i)))
+        core_stage(b, 0, turn(0))
         hook("core")
-        loop(n_fs, lambda i: y_stage(b, turn(i)))
+
+        def ahead(i):
+            pl.when(i < last)(lambda: core_stage(b, 0, turn(i + 1)))
+            y_stage(b, turn(i))
+
+        loop(n_fs, ahead)
         loop(n_fs, lambda i: core_stage(b, 1, turn(i)))
         for kk in range(n_fs):
             z_stage(b, turn(kk))

time: 176 us -> 176 us (level)
  no operation moved by 1% of the time
where the time goes in v3:
time: 176 us
  Pallas kernels  174 us (99%)
    pallas_call x1, Pallas kernels, body_kernel(): pl.pallas_call(functools.partial(both_blocks, n_fs, n_tp, tiles, PARTS),...  174 us

profile of v3, /device:TPU:0, one launch (start us, length us, event | category | flops | bytes accessed | tf_op | source)
XLA Modules:
  0.0 175.6 jit_solution(4524290711786503091)
XLA Ops:
  0.0 173.9 %shard_map.145 = bf16[256,512]{1,0:T(8,128)(2,1)} custom-call(bf16[256,512]{1,0:T(8,128)(2,1)} %refs_0_.1, f32[1,512]{1,0:T(1,128)} %bitcast.4, f32[1408]{0:T(1024)} %refs_2_.1, f32[1408]{0:T(1024)} %refs_3_.1, f32[1,512]{1,0:T(1,128)} %bitcast.5, f32[1,512]{1,0:T(1,128)} %bitcast.6, f32[1408]{0:T(1024)} %refs_6_.1, f32[1408]{0:T(1024)} %refs_7_.1, ...), custom_call_target="tpu_custom_call" | custom-call | tf_op jit(solution)/shard_map/pallas_call | solution.py:633
  173.9 1.7 copy.17
